TPU v7x, 32 devices: a whole 2x2x4 slice. The times are simulated.
32 devices in a mesh: fs: 4 (over y, x), tp: 8 (over z, core).
Axes of the slice: x: 2, y: 2, z: 4, core: 2. Of those that a mesh axis runs over, the one named last changes fastest.
Arguments:
- normed_inputs: bfloat16 [4096, 4096], P('fs', 'tp'), may hold values from -6 to 6
- query_upstream: bfloat16 [4096, 4096], P('fs', 'tp'), may hold values from -0.125 to 0.125
- key_upstream: bfloat16 [4096, 1024], P('fs', 'tp'), may hold values from -0.09375 to 0.09375
- head_outputs: bfloat16 [4096, 4096], P('fs', 'tp'), may hold values from -6 to 6
- branch_upstream: bfloat16 [4096, 4096], P('fs', 'tp'), may hold values from -0.125 to 0.125
- query_master: float32 [4096, 4096], P('fs', 'tp'), may hold values from -0.09375 to 0.09375
- key_master: float32 [4096, 1024], P('fs', 'tp'), may hold values from -0.09375 to 0.09375
- branch_master: float32 [4096, 4096], P('fs', 'tp'), may hold values from -0.09375 to 0.09375
- query_basis: bfloat16 [4096, 128], replicated, may hold values from -0.09375 to 0.09375
- key_basis: bfloat16 [4096, 128], replicated, may hold values from -0.09375 to 0.09375
- branch_basis: bfloat16 [4096, 128], replicated, may hold values from -0.09375 to 0.09375
- query_first: float32 [128, 4096], P(None, 'tp'), may hold values from -0.75 to 0.75
- query_second: float32 [128, 4096], P(None, 'tp'), may hold values from 0.001 to 0.02
- key_first: float32 [128, 1024], P(None, 'tp'), may hold values from -0.75 to 0.75
- key_second: float32 [128, 1024], P(None, 'tp'), may hold values from 0.001 to 0.02
- branch_first: float32 [4096, 128], P('fs'), may hold values from -0.75 to 0.75
- branch_second: float32 [4096, 128], P('fs'), may hold values from 0.001 to 0.02
Outputs:
- query_step: float32 [4096, 4096], P('fs', 'tp')
- key_step: float32 [4096, 1024], P('fs', 'tp')
- branch_step: float32 [4096, 4096], P('fs', 'tp')
- query_updated: float32 [4096, 4096], P('fs', 'tp')
- key_updated: float32 [4096, 1024], P('fs', 'tp')
- branch_updated: float32 [4096, 4096], P('fs', 'tp')
- query_copy: bfloat16 [4096, 4096], P(None, 'tp')
- key_copy: bfloat16 [4096, 1024], P(None, 'tp')
- branch_copy: bfloat16 [4096, 4096], P(None, 'tp')
- query_first_new: float32 [128, 4096], P(None, 'tp')
- query_second_new: float32 [128, 4096], P(None, 'tp')
- key_first_new: float32 [128, 1024], P(None, 'tp')
- key_second_new: float32 [128, 1024], P(None, 'tp')
- branch_first_new: float32 [4096, 128], P('fs')
- branch_second_new: float32 [4096, 128], P('fs')
All inputs are finite; a program needn't handle non-finite values.
Results may differ from a plain program's by a relative error of at most 0.001.
Values may be sent and summed in bfloat16 or wider, within the bound.
No kernel may reach another device: no remote copies, remote signals or barrier semaphores. Data moves between devices by JAX's collectives and lax.ppermute only.
A program may use at most 128 MiB of HBM per device.

v0:
```python
import jax
import jax.numpy as jnp
from jax import lax
from jax.sharding import PartitionSpec as P

LEARN = 0.02
BETA_ONE = 0.9
BETA_TWO = 0.95
ADAM_EPS = 1e-08
CLIP_RMS = 0.5


def moments(first, second, low, clip):
    scaled = clip * low
    first_new = BETA_ONE * first + (1.0 - BETA_ONE) * scaled
    second_new = BETA_TWO * second + (1.0 - BETA_TWO) * scaled * scaled
    return (first_new, second_new, first_new / (jnp.sqrt(second_new) + ADAM_EPS))


def over_tokens(left, right, precision=None):
    return lax.dot_general(
        left,
        right,
        (((0,), (0,)), ((), ())),
        precision=precision,
        preferred_element_type=jnp.float32,
    )


def per_device(
    normed_inputs,
    query_upstream,
    key_upstream,
    head_outputs,
    branch_upstream,
    query_master,
    key_master,
    branch_master,
    query_basis,
    key_basis,
    branch_basis,
    query_first,
    query_second,
    key_first,
    key_second,
    branch_first,
    branch_second,
):
    exact = lax.Precision.HIGHEST
    row_index = lax.axis_index("fs")
    col_index = lax.axis_index("tp")
    n_rows = lax.axis_size("fs")
    n_cols = lax.axis_size("tp")
    features = normed_inputs.shape[1]
    query_local = query_upstream.shape[1]
    key_local = key_upstream.shape[1]
    rows_in = query_master.shape[0]
    rank = query_basis.shape[1]
    whole_values = lax.all_gather(head_outputs, "tp", axis=1, tiled=True)
    block_query = lax.dynamic_slice_in_dim(query_basis, col_index * features, features, 0)
    block_key = lax.dynamic_slice_in_dim(key_basis, col_index * features, features, 0)
    proj_query, proj_key = lax.psum(
        (
            jnp.dot(normed_inputs, block_query, preferred_element_type=jnp.float32),
            jnp.dot(normed_inputs, block_key, preferred_element_type=jnp.float32),
        ),
        "tp",
    )
    part_query = over_tokens(proj_query, query_upstream.astype(jnp.float32), exact)
    part_key = over_tokens(proj_key, key_upstream.astype(jnp.float32), exact)
    grad_branch = lax.psum_scatter(
        over_tokens(whole_values, branch_upstream), "fs", scatter_dimension=0, tiled=True
    )
    own_branch = lax.dynamic_slice_in_dim(branch_basis, col_index * features, features, 0).astype(
        jnp.float32
    )
    part_branch = jnp.dot(grad_branch, own_branch, precision=exact)
    query_low, key_low = lax.psum((part_query, part_key), "fs")
    branch_low = lax.psum(part_branch, "tp")
    local_squares = (jnp.sum(query_low * query_low) + jnp.sum(key_low * key_low)) / n_rows
    local_squares = local_squares + jnp.sum(branch_low * branch_low) / n_cols
    total = lax.psum(local_squares, ("fs", "tp"))
    entries = rank * n_cols * (2 * query_local + key_local)
    rms_value = jnp.sqrt(total / float(entries))
    clip = 1.0 / jnp.maximum(1.0, rms_value / CLIP_RMS)
    q_first, q_second, q_dir = moments(query_first, query_second, query_low, clip)
    k_first, k_second, k_dir = moments(key_first, key_second, key_low, clip)
    b_first, b_second, b_dir = moments(branch_first, branch_second, branch_low, clip)
    step_rows_query = lax.dynamic_slice_in_dim(query_basis, row_index * rows_in, rows_in, 0).astype(
        jnp.float32
    )
    step_rows_key = lax.dynamic_slice_in_dim(key_basis, row_index * rows_in, rows_in, 0).astype(
        jnp.float32
    )
    query_step = jnp.dot(step_rows_query, q_dir, precision=exact)
    key_step = jnp.dot(step_rows_key, k_dir, precision=exact)
    branch_step = jnp.dot(b_dir, own_branch.T, precision=exact)
    query_updated = query_master - LEARN * query_step
    key_updated = key_master - LEARN * key_step
    branch_updated = branch_master - LEARN * branch_step
    query_copy, key_copy, branch_copy = (
        lax.all_gather(query_updated.astype(jnp.bfloat16), "fs", axis=0, tiled=True),
        lax.all_gather(key_updated.astype(jnp.bfloat16), "fs", axis=0, tiled=True),
        lax.all_gather(branch_updated.astype(jnp.bfloat16), "fs", axis=0, tiled=True),
    )
    return (
        query_step,
        key_step,
        branch_step,
        query_updated,
        key_updated,
        branch_updated,
        query_copy,
        key_copy,
        branch_copy,
        q_first,
        q_second,
        k_first,
        k_second,
        b_first,
        b_second,
    )


def solution(mesh):
    return jax.shard_map(
        per_device,
        mesh=mesh,
        in_specs=(
            P("fs", "tp"),
            P("fs", "tp"),
            P("fs", "tp"),
            P("fs", "tp"),
            P("fs", "tp"),
            P("fs", "tp"),
            P("fs", "tp"),
            P("fs", "tp"),
            P(),
            P(),
            P(),
            P(None, "tp"),
            P(None, "tp"),
            P(None, "tp"),
            P(None, "tp"),
            P("fs", None),
            P("fs", None),
        ),
        out_specs=(
            P("fs", "tp"),
            P("fs", "tp"),
            P("fs", "tp"),
            P("fs", "tp"),
            P("fs", "tp"),
            P("fs", "tp"),
            P(None, "tp"),
            P(None, "tp"),
            P(None, "tp"),
            P(None, "tp"),
            P(None, "tp"),
            P(None, "tp"),
            P(None, "tp"),
            P("fs", None),
            P("fs", None),
        ),
        check_vma=False,
    )
```

profile of v0, /device:TPU:0, one launch (start us, length us, event | category | flops | bytes accessed | tf_op | source)
XLA Modules:
  0.0 502.3 jit_solution(1356573704103843505)
XLA Ops:
  7.2 0.7 all-gather.5.cloned.1.call-update
  8.0 86.4 %all-gather.5.cloned.1.call-done = bf16[1024,4096]{1,0:T(8,128)(2,1)} async-done(((bf16[1024,512]{1,0:T(8,128)(2,1)}), bf16[1024,4096]{1,0:T(8,128)(2,1)}) %all-gather.5.cloned.1.call-update) | async-done | bytes 8388624 | tf_op jit(solution)/shard_map/all_gather | solution.py:59
  94.4 10.4 %fusion.39 = f32[4096,512]{1,0:T(8,128)} fusion(bf16[1024,4096]{1,0:T(8,128)(2,1)} %all-gather.5.cloned.1.call-done, bf16[1024,512]{1,0:T(8,128)(2,1)S(1)} %copy-done), kind=kOutput, calls=%fused_computation.53 | convolution fusion | flops 4294967296 | bytes 17825792 | tf_op jit(solution)/shard_map/dot_general | solution.py:21
  104.9 0.0 all-reduce.5.cloned.1.call-start
  104.9 1.1 copy-done.2
  106.1 2.2 convolution_bitcast_fusion
  108.2 2.2 convolution_bitcast_fusion.1
  110.4 79.4 %reduce-scatter.2.cloned.1.call-done = f32[1024,512]{1,0:T(8,128)} async-done(((f32[4096,512]{1,0:T(8,128)}), f32[1024,512]{1,0:T(8,128)}) %reduce-scatter.2.cloned.1.call-update) | async-done | bytes 2097168 | tf_op jit(solution)/shard_map/reduce_scatter | solution.py:71
  189.8 3.4 fusion.18
  193.3 0.0 all-reduce.7.cloned.1.call-start
  193.4 62.4 %all-reduce.5.cloned.1.call-done = (f32[1024,128]{0,1:T(8,128)}, f32[1024,128]{0,1:T(8,128)}, f32[1024,128]{1,0:T(8,128)}) async-done(((f32[1024,128]{0,1:T(8,128)}, f32[1024,128]{0,1:T(8,128)}, f32[1024,128]{1,0:T(8,128)}), (f32[1024,128]{0,1:T(8,128)}, f32[1024,128]{0,1:T(8,128)}, f32[1024,128]{1,0:T(8,128)})) %all-reduce.5.cloned.1.call-update) | async-done | bytes 1572880 | tf_op jit(solution)/shard_map/psum | solution.py:62
  255.8 2.5 fusion.37
  258.3 1.0 fusion.38
  259.3 0.0 all-gather.9.cloned.1.call-start
  259.4 0.7 multiply_reduce_fusion
  260.7 41.6 %all-reduce.7.cloned.1.call-done = (f32[128,512]{1,0:T(8,128)}, f32[128,128]{1,0:T(8,128)}) async-done(((f32[128,512]{1,0:T(8,128)}, f32[128,128]{1,0:T(8,128)}), (f32[128,512]{1,0:T(8,128)}, f32[128,128]{1,0:T(8,128)})) %all-reduce.7.cloned.1.call-update) | async-done | bytes 327696 | tf_op jit(solution)/shard_map/psum | solution.py:78
  302.3 1.6 multiply_reduce_fusion.1
  303.9 1.5 multiply_reduce_fusion.2
  306.7 39.3 %psum.47 = f32[]{:T(128)} all-reduce(f32[]{:T(128)S(6)} %add.68), channel_id=1, replica_groups=mesh['fs'=4,'tp'=8] {'fs','tp'}, use_global_device_ids=true, to_apply=%region_9.0 | all-reduce | flops 1 | bytes 8 | tf_op jit(solution)/shard_map/psum | solution.py:82
  346.8 0.9 fusion.20
  347.7 2.6 fusion.35
  350.3 1.4 fusion
  351.7 4.7 fusion.34
  356.5 1.2 fusion.5
  357.7 0.4 copy-done.8
  358.1 4.5 fusion.36
  362.7 15.2 %all-gather.9.cloned.1.call-done = bf16[4096,128]{1,0:T(8,128)(2,1)} async-done(((bf16[1024,128]{1,0:T(8,128)(2,1)}), bf16[4096,128]{1,0:T(8,128)(2,1)}) %all-gather.9.cloned.1.call-update) | async-done | bytes 1048592 | tf_op jit(solution)/shard_map/all_gather | solution.py:103
  377.9 54.9 %all-gather.11.cloned.1.call-done = bf16[4096,512]{1,0:T(8,128)(2,1)} async-done(((bf16[1024,512]{1,0:T(8,128)(2,1)}), bf16[4096,512]{1,0:T(8,128)(2,1)}) %all-gather.11.cloned.1.call-update) | async-done | bytes 4194320 | tf_op jit(solution)/shard_map/all_gather | solution.py:104
  432.8 55.0 %all-gather.7.cloned.1.call-done = bf16[4096,512]{1,0:T(8,128)(2,1)} async-done(((bf16[1024,512]{1,0:T(8,128)(2,1)}), bf16[4096,512]{1,0:T(8,128)(2,1)}) %all-gather.7.cloned.1.call-update) | async-done | bytes 4194320 | tf_op jit(solution)/shard_map/all_gather | solution.py:102
  487.8 4.6 copy.40
  492.5 1.0 copy.41
  493.4 2.0 copy.42
  (52 shorter events, 0.4 us)
Async XLA Ops:
  7.2 87.2 %copy-start = (bf16[1024,512]{1,0:T(8,128)(2,1)S(1)}, bf16[1024,512]{1,0:T(8,128)(2,1)}, u32[]{:S(2)}) copy-start(bf16[1024,512]{1,0:T(8,128)(2,1)} %param.21) | copy-start | bytes 3145732
  7.2 87.2 %all-gather.5.cloned.1.call-start = ((), (), s32[]{:S(2)}) async-start(), calls=%async_computation.1 | async-start | bytes 9437184 | tf_op jit(solution)/shard_map/all_gather | solution.py:59
  7.9 181.9 %reduce-scatter.2.cloned.1.call-start = ((), (), s32[]{:S(2)}) async-start(), calls=%async_computation.2 | async-start | bytes 10485760 | tf_op jit(solution)/shard_map/reduce_scatter | solution.py:71
  104.9 1.2 copy-start.2
  104.9 150.9 %all-reduce.5.cloned.1.call-start = ((), (), s32[]{:S(2)}) async-start(), calls=%async_computation.6 | async-start | bytes 3145728 | tf_op jit(solution)/shard_map/psum | solution.py:62
  110.4 145.4 %copy-start.11 = (bf16[1024,512]{1,0:T(8,128)(2,1)S(1)}, bf16[1024,512]{1,0:T(8,128)(2,1)}, u32[]{:S(2)}) copy-start(bf16[1024,512]{1,0:T(8,128)(2,1)} %param.18) | copy-start | bytes 3145732
  193.3 65.0 %copy-start.19 = (bf16[1024,128]{1,0:T(8,128)(2,1)S(1)}, bf16[1024,128]{1,0:T(8,128)(2,1)}, u32[]{:S(2)}) copy-start(bf16[1024,128]{1,0:T(8,128)(2,1)} %param.19) | copy-start | bytes 786436
  193.3 153.5 %copy-start.20 = (f32[128,128]{1,0:T(8,128)S(1)}, f32[128,128]{1,0:T(8,128)}, u32[]{:S(2)}) copy-start(f32[128,128]{1,0:T(8,128)} %param.31) | copy-start | bytes 196612
  193.3 153.5 %copy-start.21 = (f32[128,128]{1,0:T(8,128)S(1)}, f32[128,128]{1,0:T(8,128)}, u32[]{:S(2)}) copy-start(f32[128,128]{1,0:T(8,128)} %param.30) | copy-start | bytes 196612
  193.3 109.0 %all-reduce.7.cloned.1.call-start = ((), (), s32[]{:S(2)}) async-start(), calls=%async_computation.7 | async-start | bytes 655360 | tf_op jit(solution)/shard_map/psum | solution.py:78
  255.8 2.5 copy-start.15
  255.8 3.6 copy-start.6
  255.8 91.9 %copy-start.14 = (f32[1024,128]{1,0:T(8,128)S(1)}, f32[1024,128]{1,0:T(8,128)}, u32[]{:S(2)}) copy-start(f32[1024,128]{1,0:T(8,128)} %param.23) | copy-start | bytes 1572868
  259.3 118.6 %all-gather.9.cloned.1.call-start = ((), (), s32[]{:S(2)}) async-start(), calls=%async_computation.4 | async-start | bytes 1310720 | tf_op jit(solution)/shard_map/all_gather | solution.py:103
  347.6 4.0 copy-start.17
  347.6 4.0 copy-start.18
  347.7 4.0 copy-start.7
  350.3 82.5 %all-gather.11.cloned.1.call-start = ((), (), s32[]{:S(2)}) async-start(), calls=%async_computation.5 | async-start | bytes 5242880 | tf_op jit(solution)/shard_map/all_gather | solution.py:104
  351.7 4.7 copy-start.4
  351.7 4.7 copy-start.5
  351.7 4.8 copy-start.12
  351.7 4.8 copy-start.16
  356.4 1.7 copy-start.8
  356.4 131.4 %all-gather.7.cloned.1.call-start = ((), (), s32[]{:S(2)}) async-start(), calls=%async_computation.3 | async-start | bytes 5242880 | tf_op jit(solution)/shard_map/all_gather | solution.py:102
  357.7 5.0 copy-start.9
  357.7 5.0 copy-start.10
  487.8 4.6 copy-start.13
  487.8 5.6 %copy-start.3 = (bf16[4096,512]{1,0:T(8,128)(2,1)S(1)}, bf16[4096,512]{1,0:T(8,128)(2,1)}, u32[]{:S(2)}) copy-start(bf16[4096,512]{1,0:T(8,128)(2,1)} %all-gather.11.cloned.1.call-done) | copy-start | bytes 12582916
  493.4 2.0 copy-start.1
Sparse Core Ops, SparseCore 0:
  9.6 84.7 all-gather.4
  105.0 84.7 reduce-scatter.1
  193.6 62.1 all-reduce.4
  259.4 42.8 all-reduce.6
  350.4 27.4 all-gather.8
  380.2 52.5 all-gather.10
  435.2 52.5 all-gather.6
where the time goes:
time: 503 us; the launch traced here: 502 us
  waiting for transfers between devices  396 us (79%)
  blocking collectives  39.3 us (8%)
  matrix products  33.4 us (7%)
  between operations  17 us (3%)
  local copies, waits for them, and re-layouts  9.28 us (2%)
  other arithmetic  7.2 us (1%)
    all_gather x1, waiting for transfers between devices, per_device(): whole_values = lax.all_gather(head_outputs, 'tp', axis=1, tiled=True)  86.4 us
    reduce_scatter x1, waiting for transfers between devices, per_device(): lax.psum_scatter(over_tokens(whole_values, branch_upstream), 'fs', scatte...  79.4 us
    psum x1, waiting for transfers between devices, per_device(): lax.psum((jnp.dot(normed_inputs, block_query, preferred_element_type=jnp....  62.4 us
    all_gather x1, waiting for transfers between devices, per_device(): lax.all_gather(query_updated.astype(jnp.bfloat16), 'fs', axis=0, tiled=True)  55 us
    all_gather x1, waiting for transfers between devices, per_device(): lax.all_gather(branch_updated.astype(jnp.bfloat16), 'fs', axis=0, tiled=T...  54.9 us
    psum x1, waiting for transfers between devices, per_device(): query_low, key_low = lax.psum((part_query, part_key), 'fs')  41.6 us
    psum x1, blocking collectives, per_device(): total = lax.psum(local_squares, ('fs', 'tp'))  39.3 us
    all_gather x1, waiting for transfers between devices, per_device(): lax.all_gather(key_updated.astype(jnp.bfloat16), 'fs', axis=0, tiled=True)  15.2 us
  transfers between devices with their start and end apart: 7, of which 7 were waited for; matrix products, arithmetic and copies ran while one was open for 3% of the time, Pallas kernels for 0%

commit v1 on v0

--- a/solution.py
+++ b/solution.py
@@ -8,6 +8,20 @@
 BETA_TWO = 0.95
 ADAM_EPS = 1e-08
 CLIP_RMS = 0.5
+
+
+def _bind_lines(shard_in):
+    mesh_dim = "tp"
+    windows = [shard_in]
+    world = lax.axis_size(mesh_dim)
+    for src_i in [*range(world - 1)]:
+        main = lax.ppermute(
+            windows[-1], axis_name=mesh_dim, perm=[(j, (j + 1) % world) for j in range(world)]
+        )
+        windows.append(main)
+    taken_in = jnp.concatenate(windows[::-1], axis=1)
+    frame_out = lax.axis_index(mesh_dim)
+    return jnp.roll(taken_in, (frame_out + 1) * shard_in.shape[1], axis=1)
 
 
 def moments(first, second, low, clip):
@@ -56,7 +70,7 @@
     key_local = key_upstream.shape[1]
     rows_in = query_master.shape[0]
     rank = query_basis.shape[1]
-    whole_values = lax.all_gather(head_outputs, "tp", axis=1, tiled=True)
+    whole_values = _bind_lines(head_outputs)
     block_query = lax.dynamic_slice_in_dim(query_basis, col_index * features, features, 0)
     block_key = lax.dynamic_slice_in_dim(key_basis, col_index * features, features, 0)
     proj_query, proj_key = lax.psum(

time: 503 us -> 548 us (1.089)
  waiting for transfers between devices: 396 us -> 421 us
  local copies, waits for them, and re-layouts: 9.28 us -> 28.2 us
    ppermute x0 -> x7, waiting for transfers between devices: none -> 113 us  [_bind_lines(): lax.ppermute(windows[-1], axis_name=mesh_dim, perm=[(j, (j + 1) % world)...]
    all_gather x1 -> x0, waiting for transfers between devices: 86.4 us -> none  [per_device(): whole_values = lax.all_gather(head_outputs, 'tp', axis=1, tiled=True)]
    unnamed x47 -> x68, local copies, waits for them, and re-layouts: 9.28 us -> 28.1 us
  transfers between devices with their start and end apart: 7 -> 13, of which waited for: 7 -> 13; matrix products, arithmetic and copies ran while one was open for 3% -> 4% of each run, Pallas kernels for 0% -> 0%
where the time goes in v1:
time: 548 us; the launch traced here: 547 us
  waiting for transfers between devices  421 us (77%)
  blocking collectives  39.3 us (7%)
  matrix products  32.8 us (6%)
  local copies, waits for them, and re-layouts  28.2 us (5%)
  between operations  17.2 us (3%)
  other arithmetic  8.13 us (1%)
    ppermute x7, waiting for transfers between devices, _bind_lines(): lax.ppermute(windows[-1], axis_name=mesh_dim, perm=[(j, (j + 1) % world)...  113 us
    reduce_scatter x1, waiting for transfers between devices, per_device(): lax.psum_scatter(over_tokens(whole_values, branch_upstream), 'fs', scatte...  80.7 us
    psum x1, waiting for transfers between devices, per_device(): lax.psum((jnp.dot(normed_inputs, block_query, preferred_element_type=jnp....  62.5 us
    all_gather x1, waiting for transfers between devices, per_device(): lax.all_gather(query_updated.astype(jnp.bfloat16), 'fs', axis=0, tiled=True)  54.9 us
    all_gather x1, waiting for transfers between devices, per_device(): lax.all_gather(branch_updated.astype(jnp.bfloat16), 'fs', axis=0, tiled=T...  54.9 us
    psum x1, waiting for transfers between devices, per_device(): query_low, key_low = lax.psum((part_query, part_key), 'fs')  40.5 us
    psum x1, blocking collectives, per_device(): total = lax.psum(local_squares, ('fs', 'tp'))  39.3 us
    unnamed x68, local copies, waits for them, and re-layouts  28.1 us
  transfers between devices with their start and end apart: 13, of which 13 were waited for; matrix products, arithmetic and copies ran while one was open for 4% of the time, Pallas kernels for 0%

profile of v1, /device:TPU:0, one launch (start us, length us, event | category | flops | bytes accessed | tf_op | source)
XLA Modules:
  0.0 547.2 jit_solution(6530817916398425807)
XLA Ops:
  7.8 16.7 %collective-permute-done = bf16[1024,512]{1,0:T(8,128)(2,1)S(1)} collective-permute-done((bf16[1024,512]{1,0:T(8,128)(2,1)}, bf16[1024,512]{1,0:T(8,128)(2,1)S(1)}, u32[]{:S(2)}, u32[]{:S(2)}) %collective-permute-start) | collective-permute-done | bytes 1048608 | tf_op jit(solution)/shard_map/ppermute | solution.py:18
  24.5 16.0 %collective-permute-done.1 = bf16[1024,512]{1,0:T(8,128)(2,1)S(1)} collective-permute-done((bf16[1024,512]{1,0:T(8,128)(2,1)S(1)}, bf16[1024,512]{1,0:T(8,128)(2,1)S(1)}, u32[]{:S(2)}, u32[]{:S(2)}) %collective-permute-start.1) | collective-permute-done | bytes 1048608 | tf_op jit(solution)/shard_map/ppermute | solution.py:18
  41.5 16.0 %collective-permute-done.2 = bf16[1024,512]{1,0:T(8,128)(2,1)S(1)} collective-permute-done((bf16[1024,512]{1,0:T(8,128)(2,1)S(1)}, bf16[1024,512]{1,0:T(8,128)(2,1)S(1)}, u32[]{:S(2)}, u32[]{:S(2)}) %collective-permute-start.2) | collective-permute-done | bytes 1048608 | tf_op jit(solution)/shard_map/ppermute | solution.py:18
  58.5 16.0 %collective-permute-done.3 = bf16[1024,512]{1,0:T(8,128)(2,1)S(1)} collective-permute-done((bf16[1024,512]{1,0:T(8,128)(2,1)S(1)}, bf16[1024,512]{1,0:T(8,128)(2,1)S(1)}, u32[]{:S(2)}, u32[]{:S(2)}) %collective-permute-start.3) | collective-permute-done | bytes 1048608 | tf_op jit(solution)/shard_map/ppermute | solution.py:18
  75.5 16.0 %collective-permute-done.4 = bf16[1024,512]{1,0:T(8,128)(2,1)S(1)} collective-permute-done((bf16[1024,512]{1,0:T(8,128)(2,1)S(1)}, bf16[1024,512]{1,0:T(8,128)(2,1)S(1)}, u32[]{:S(2)}, u32[]{:S(2)}) %collective-permute-start.4) | collective-permute-done | bytes 1048608 | tf_op jit(solution)/shard_map/ppermute | solution.py:18
  92.5 16.1 %collective-permute-done.5 = bf16[1024,512]{1,0:T(8,128)(2,1)} collective-permute-done((bf16[1024,512]{1,0:T(8,128)(2,1)S(1)}, bf16[1024,512]{1,0:T(8,128)(2,1)}, u32[]{:S(2)}, u32[]{:S(2)}) %collective-permute-start.5) | collective-permute-done | bytes 1048608 | tf_op jit(solution)/shard_map/ppermute | solution.py:18
  108.6 16.3 %collective-permute-done.6 = bf16[1024,512]{1,0:T(8,128)(2,1)} collective-permute-done((bf16[1024,512]{1,0:T(8,128)(2,1)}, bf16[1024,512]{1,0:T(8,128)(2,1)}, u32[]{:S(2)}, u32[]{:S(2)}) %collective-permute-start.6) | collective-permute-done | bytes 1048608 | tf_op jit(solution)/shard_map/ppermute | solution.py:18
  126.3 1.3 constant_dynamic-update-slice_fusion.14
  130.4 1.3 constant_dynamic-update-slice_fusion.11
  138.2 7.0 %fusion = f32[4096,512]{1,0:T(8,128)} fusion(bf16[1024,512]{1,0:T(8,128)(2,1)S(1)} %copy-done, bf16[1024,8192]{1,0:T(8,128)(2,1)S(1)} %constant_dynamic-update-slice_fusion, s32[]{:T(128)S(6)} %select_n.25), kind=kOutput, calls=%fused_computation | convolution fusion | flops 4294967296 | bytes 17825796 | tf_op jit(solution)/shard_map/dot_general | solution.py:35
  145.3 2.3 convolution_bitcast_fusion
  147.6 2.2 convolution_bitcast_fusion.1
  149.7 80.7 %reduce-scatter.2.cloned.1.call-done = f32[1024,512]{1,0:T(8,128)} async-done(((f32[4096,512]{1,0:T(8,128)}), f32[1024,512]{1,0:T(8,128)}) %reduce-scatter.2.cloned.1.call-update) | async-done | bytes 2097168 | tf_op jit(solution)/shard_map/reduce_scatter | solution.py:85
  230.4 3.4 fusion.20
  233.9 62.5 %all-reduce.5.cloned.1.call-done = (f32[1024,128]{0,1:T(8,128)}, f32[1024,128]{0,1:T(8,128)}, f32[1024,128]{1,0:T(8,128)}) async-done(((f32[1024,128]{0,1:T(8,128)}, f32[1024,128]{0,1:T(8,128)}, f32[1024,128]{1,0:T(8,128)}), (f32[1024,128]{0,1:T(8,128)}, f32[1024,128]{0,1:T(8,128)}, f32[1024,128]{1,0:T(8,128)})) %all-reduce.5.cloned.1.call-update) | async-done | bytes 1572880 | tf_op jit(solution)/shard_map/psum | solution.py:76
  296.4 2.3 fusion.40
  298.8 2.2 fusion.41
  301.0 1.8 multiply_reduce_fusion
  303.4 40.5 %all-reduce.7.cloned.1.call-done = (f32[128,512]{1,0:T(8,128)}, f32[128,128]{1,0:T(8,128)}) async-done(((f32[128,512]{1,0:T(8,128)}, f32[128,128]{1,0:T(8,128)}), (f32[128,512]{1,0:T(8,128)}, f32[128,128]{1,0:T(8,128)})) %all-reduce.7.cloned.1.call-update) | async-done | bytes 327696 | tf_op jit(solution)/shard_map/psum | solution.py:92
  344.0 1.6 multiply_reduce_fusion.1
  345.6 1.5 multiply_reduce_fusion.2
  348.3 39.3 %psum.47 = f32[]{:T(128)} all-reduce(f32[]{:T(128)S(6)} %add.84), channel_id=1, replica_groups=mesh['fs'=4,'tp'=8] {'fs','tp'}, use_global_device_ids=true, to_apply=%region_9.10 | all-reduce | flops 1 | bytes 8 | tf_op jit(solution)/shard_map/psum | solution.py:96
  389.3 2.4 fusion.38
  391.8 1.4 fusion.2
  393.2 5.5 %fusion.37 = (bf16[1024,512]{1,0:T(8,128)(2,1)}, f32[1024,512]{1,0:T(8,128)}, f32[1024,512]{1,0:T(8,128)}) fusion(f32[1024,512]{1,0:T(8,128)} %param.24, bf16[4096,128]{1,0:T(8,128)(2,1)} %param.27, s32[]{:T(128)S(6)} %select_n.23, f32[1024,128]{1,0:T(8,128)S(1)} %get-tuple-element.63, f32[1024,128]{1,0:T(8,128)S(1)} %get-tuple-element.64), kind=kOutput, calls=%fused_computation.67 | convolution fusion | flops 807141376 | bytes 8519684 | tf_op jit(solution)/shard_map/dot_general | solution.py:111
  399.9 5.5 %fusion.39 = (bf16[1024,512]{1,0:T(8,128)(2,1)}, f32[1024,512]{1,0:T(8,128)}, f32[1024,512]{1,0:T(8,128)}) fusion(f32[1024,512]{1,0:T(8,128)} %param.22, f32[128,512]{1,0:T(8,128)S(1)} %get-tuple-element.59, f32[128,512]{1,0:T(8,128)S(1)} %get-tuple-element.60, bf16[4096,128]{1,0:T(8,128)(2,1)} %param.25, s32[]{:T(128)S(6)} %select_n.22), kind=kOutput, calls=%fused_computation.69 | convolution fusion | flops 807010304 | bytes 8126468 | tf_op jit(solution)/shard_map/dot_general | solution.py:109
  405.4 13.9 %all-gather.6.cloned.1.call-done = bf16[4096,128]{1,0:T(8,128)(2,1)} async-done(((bf16[1024,128]{1,0:T(8,128)(2,1)}), bf16[4096,128]{1,0:T(8,128)(2,1)}) %all-gather.6.cloned.1.call-update) | async-done | bytes 1048592 | tf_op jit(solution)/shard_map/all_gather | solution.py:117
  419.4 54.9 %all-gather.8.cloned.1.call-done = bf16[4096,512]{1,0:T(8,128)(2,1)} async-done(((bf16[1024,512]{1,0:T(8,128)(2,1)}), bf16[4096,512]{1,0:T(8,128)(2,1)}) %all-gather.8.cloned.1.call-update) | async-done | bytes 4194320 | tf_op jit(solution)/shard_map/all_gather | solution.py:118
  474.2 54.9 %all-gather.4.cloned.1.call-done = bf16[4096,512]{1,0:T(8,128)(2,1)} async-done(((bf16[1024,512]{1,0:T(8,128)(2,1)}), bf16[4096,512]{1,0:T(8,128)(2,1)}) %all-gather.4.cloned.1.call-update) | async-done | bytes 4194320 | tf_op jit(solution)/shard_map/all_gather | solution.py:116
  529.1 4.5 copy.55
  533.6 2.3 copy.56
  535.8 4.5 copy.57
  (85 shorter events, 17.1 us)
Async XLA Ops:
  7.2 130.9 %copy-start = (bf16[1024,512]{1,0:T(8,128)(2,1)S(1)}, bf16[1024,512]{1,0:T(8,128)(2,1)}, u32[]{:S(2)}) copy-start(bf16[1024,512]{1,0:T(8,128)(2,1)} %param.21) | copy-start | bytes 3145732
  7.2 130.8 %copy-start.3 = (bf16[1024,512]{1,0:T(8,128)(2,1)S(1)}, bf16[1024,512]{1,0:T(8,128)(2,1)}, u32[]{:S(2)}) copy-start(bf16[1024,512]{1,0:T(8,128)(2,1)} %param.20) | copy-start | bytes 3145732
  7.2 223.2 %reduce-scatter.2.cloned.1.call-start = ((), (), s32[]{:S(2)}) async-start(), calls=%async_computation.1 | async-start | bytes 10485760 | tf_op jit(solution)/shard_map/reduce_scatter | solution.py:85
  7.3 17.3 %collective-permute-start = (bf16[1024,512]{1,0:T(8,128)(2,1)}, bf16[1024,512]{1,0:T(8,128)(2,1)S(1)}, u32[]{:S(2)}, u32[]{:S(2)}) collective-permute-start(bf16[1024,512]{1,0:T(8,128)(2,1)} %param.20), channel_id=1, source_target_pairs={{0,1},{1,2},{2,3},{3,4},{4,5},{5,6},{6,7},{7,0},{8,9},{9,10},{10,1... | collective-permute-start | bytes 3145736 | tf_op jit(solution)/shard_map/ppermute | solution.py:18
  24.5 16.0 %collective-permute-start.1 = (bf16[1024,512]{1,0:T(8,128)(2,1)S(1)}, bf16[1024,512]{1,0:T(8,128)(2,1)S(1)}, u32[]{:S(2)}, u32[]{:S(2)}) collective-permute-start(bf16[1024,512]{1,0:T(8,128)(2,1)S(1)} %collective-permute-done), channel_id=1, source_target_pairs={{0,1},{1,2},{2,3},{3,4},{4,5},{5,6},{6,7},{7,0},{8,9},{9,10},{10,1... | collective-permute-start | bytes 3145736 | tf_op jit(solution)/shard_map/ppermute | solution.py:18
  41.5 16.0 %collective-permute-start.2 = (bf16[1024,512]{1,0:T(8,128)(2,1)S(1)}, bf16[1024,512]{1,0:T(8,128)(2,1)S(1)}, u32[]{:S(2)}, u32[]{:S(2)}) collective-permute-start(bf16[1024,512]{1,0:T(8,128)(2,1)S(1)} %collective-permute-done.1), channel_id=1, source_target_pairs={{0,1},{1,2},{2,3},{3,4},{4,5},{5,6},{6,7},{7,0},{8,9},{9,10},{10,1... | collective-permute-start | bytes 3145736 | tf_op jit(solution)/shard_map/ppermute | solution.py:18
  58.5 16.0 %collective-permute-start.3 = (bf16[1024,512]{1,0:T(8,128)(2,1)S(1)}, bf16[1024,512]{1,0:T(8,128)(2,1)S(1)}, u32[]{:S(2)}, u32[]{:S(2)}) collective-permute-start(bf16[1024,512]{1,0:T(8,128)(2,1)S(1)} %collective-permute-done.2), channel_id=1, source_target_pairs={{0,1},{1,2},{2,3},{3,4},{4,5},{5,6},{6,7},{7,0},{8,9},{9,10},{10,1... | collective-permute-start | bytes 3145736 | tf_op jit(solution)/shard_map/ppermute | solution.py:18
  75.5 16.0 %collective-permute-start.4 = (bf16[1024,512]{1,0:T(8,128)(2,1)S(1)}, bf16[1024,512]{1,0:T(8,128)(2,1)S(1)}, u32[]{:S(2)}, u32[]{:S(2)}) collective-permute-start(bf16[1024,512]{1,0:T(8,128)(2,1)S(1)} %collective-permute-done.3), channel_id=1, source_target_pairs={{0,1},{1,2},{2,3},{3,4},{4,5},{5,6},{6,7},{7,0},{8,9},{9,10},{10,1... | collective-permute-start | bytes 3145736 | tf_op jit(solution)/shard_map/ppermute | solution.py:18
  92.5 16.1 %collective-permute-start.5 = (bf16[1024,512]{1,0:T(8,128)(2,1)S(1)}, bf16[1024,512]{1,0:T(8,128)(2,1)}, u32[]{:S(2)}, u32[]{:S(2)}) collective-permute-start(bf16[1024,512]{1,0:T(8,128)(2,1)S(1)} %collective-permute-done.4), channel_id=1, source_target_pairs={{0,1},{1,2},{2,3},{3,4},{4,5},{5,6},{6,7},{7,0},{8,9},{9,10},{10,1... | collective-permute-start | bytes 3145736 | tf_op jit(solution)/shard_map/ppermute | solution.py:18
  108.6 16.3 %collective-permute-start.6 = (bf16[1024,512]{1,0:T(8,128)(2,1)}, bf16[1024,512]{1,0:T(8,128)(2,1)}, u32[]{:S(2)}, u32[]{:S(2)}) collective-permute-start(bf16[1024,512]{1,0:T(8,128)(2,1)} %collective-permute-done.5), channel_id=1, source_target_pairs={{0,1},{1,2},{2,3},{3,4},{4,5},{5,6},{6,7},{7,0},{8,9},{9,10},{10,1... | collective-permute-start | bytes 3145736 | tf_op jit(solution)/shard_map/ppermute | solution.py:18
  108.6 28.8 %copy-start.9 = (bf16[1024,512]{1,0:T(8,128)(2,1)S(1)}, bf16[1024,512]{1,0:T(8,128)(2,1)}, u32[]{:S(2)}) copy-start(bf16[1024,512]{1,0:T(8,128)(2,1)} %copy-done.8) | copy-start | bytes 3145732
  108.6 29.0 %copy-start.7 = (bf16[1024,512]{1,0:T(8,128)(2,1)S(1)}, bf16[1024,512]{1,0:T(8,128)(2,1)}, u32[]{:S(2)}) copy-start(bf16[1024,512]{1,0:T(8,128)(2,1)} %copy-done.6) | copy-start | bytes 3145732
  108.6 29.1 %copy-start.5 = (bf16[1024,512]{1,0:T(8,128)(2,1)S(1)}, bf16[1024,512]{1,0:T(8,128)(2,1)}, u32[]{:S(2)}) copy-start(bf16[1024,512]{1,0:T(8,128)(2,1)} %copy-done.4) | copy-start | bytes 3145732
  138.1 158.3 %copy-start.16 = (bf16[1024,512]{1,0:T(8,128)(2,1)S(1)}, bf16[1024,512]{1,0:T(8,128)(2,1)}, u32[]{:S(2)}) copy-start(bf16[1024,512]{1,0:T(8,128)(2,1)} %param.18) | copy-start | bytes 3145732
  145.2 243.2 %copy-start.23 = (f32[128,128]{1,0:T(8,128)S(1)}, f32[128,128]{1,0:T(8,128)}, u32[]{:S(2)}) copy-start(f32[128,128]{1,0:T(8,128)} %param.31) | copy-start | bytes 196612
  145.2 243.2 %copy-start.24 = (f32[128,128]{1,0:T(8,128)S(1)}, f32[128,128]{1,0:T(8,128)}, u32[]{:S(2)}) copy-start(f32[128,128]{1,0:T(8,128)} %param.30) | copy-start | bytes 196612
  145.2 244.1 %copy-start.17 = (f32[1024,128]{1,0:T(8,128)S(1)}, f32[1024,128]{1,0:T(8,128)}, u32[]{:S(2)}) copy-start(f32[1024,128]{1,0:T(8,128)} %param.23) | copy-start | bytes 1572868
  145.2 246.6 %copy-start.18 = (f32[1024,128]{1,0:T(8,128)S(1)}, f32[1024,128]{1,0:T(8,128)}, u32[]{:S(2)}) copy-start(f32[1024,128]{1,0:T(8,128)} %param.33) | copy-start | bytes 1572868
  145.2 253.6 %copy-start.19 = (f32[128,512]{1,0:T(8,128)S(1)}, f32[128,512]{1,0:T(8,128)}, u32[]{:S(2)}) copy-start(f32[128,512]{1,0:T(8,128)} %param.29) | copy-start | bytes 786436
  145.2 151.2 %all-reduce.5.cloned.1.call-start = ((), (), s32[]{:S(2)}) async-start(), calls=%async_computation.5 | async-start | bytes 3145728 | tf_op jit(solution)/shard_map/psum | solution.py:76
  233.9 110.1 %all-reduce.7.cloned.1.call-start = ((), (), s32[]{:S(2)}) async-start(), calls=%async_computation.6 | async-start | bytes 655360 | tf_op jit(solution)/shard_map/psum | solution.py:92
  298.8 100.0 %copy-start.20 = (f32[128,512]{1,0:T(8,128)S(1)}, f32[128,512]{1,0:T(8,128)}, u32[]{:S(2)}) copy-start(f32[128,512]{1,0:T(8,128)} %param.28) | copy-start | bytes 786436
  300.9 118.4 %all-gather.6.cloned.1.call-start = ((), (), s32[]{:S(2)}) async-start(), calls=%async_computation.3 | async-start | bytes 1310720 | tf_op jit(solution)/shard_map/all_gather | solution.py:117
  389.3 144.3 %copy-start.21 = (f32[128,128]{1,0:T(8,128)}, f32[128,128]{1,0:T(8,128)S(1)}, u32[]{:S(2)}) copy-start(f32[128,128]{1,0:T(8,128)S(1)} %get-tuple-element.62) | copy-start | bytes 196612
  389.3 144.3 %copy-start.22 = (f32[128,128]{1,0:T(8,128)}, f32[128,128]{1,0:T(8,128)S(1)}, u32[]{:S(2)}) copy-start(f32[128,128]{1,0:T(8,128)S(1)} %get-tuple-element.61) | copy-start | bytes 196612
  391.7 82.5 %all-gather.8.cloned.1.call-start = ((), (), s32[]{:S(2)}) async-start(), calls=%async_computation.4 | async-start | bytes 5242880 | tf_op jit(solution)/shard_map/all_gather | solution.py:118
  393.2 147.2 %copy-start.12 = (f32[1024,128]{1,0:T(8,128)}, f32[1024,128]{1,0:T(8,128)S(1)}, u32[]{:S(2)}) copy-start(f32[1024,128]{1,0:T(8,128)S(1)} %get-tuple-element.64) | copy-start | bytes 1572868
  393.2 147.1 %copy-start.13 = (f32[1024,128]{1,0:T(8,128)}, f32[1024,128]{1,0:T(8,128)S(1)}, u32[]{:S(2)}) copy-start(f32[1024,128]{1,0:T(8,128)S(1)} %get-tuple-element.63) | copy-start | bytes 1572868
  393.2 147.1 %copy-start.1 = (bf16[1024,512]{1,0:T(8,128)(2,1)S(1)}, bf16[1024,512]{1,0:T(8,128)(2,1)}, u32[]{:S(2)}) copy-start(bf16[1024,512]{1,0:T(8,128)(2,1)} %param.21) | copy-start | bytes 3145732
  398.7 130.4 %all-gather.4.cloned.1.call-start = ((), (), s32[]{:S(2)}) async-start(), calls=%async_computation.2 | async-start | bytes 5242880 | tf_op jit(solution)/shard_map/all_gather | solution.py:116
  399.9 140.5 %copy-start.14 = (f32[128,512]{1,0:T(8,128)}, f32[128,512]{1,0:T(8,128)S(1)}, u32[]{:S(2)}) copy-start(f32[128,512]{1,0:T(8,128)S(1)} %get-tuple-element.60) | copy-start | bytes 786436
  399.9 140.4 %copy-start.15 = (f32[128,512]{1,0:T(8,128)}, f32[128,512]{1,0:T(8,128)S(1)}, u32[]{:S(2)}) copy-start(f32[128,512]{1,0:T(8,128)S(1)} %get-tuple-element.59) | copy-start | bytes 786436
  (6 other events, 39.7 us)
Sparse Core Ops, SparseCore 0:
  145.3 85.0 reduce-scatter.1
  234.2 62.2 all-reduce.4
  301.1 42.8 all-reduce.6
  391.9 27.4 all-gather.5
  421.6 52.5 all-gather.7
  476.5 52.5 all-gather.3
